TPU v7x, 32 devices: a whole 2x2x4 slice. The times are simulated.
32 devices in a mesh: rep: 2 (over y), fs: 4 (over z), tp: 4 (over x, core).
Axes of the slice: x: 2, y: 2, z: 4, core: 2. Of those that a mesh axis runs over, the one named last changes fastest.
Arguments:
- stream: bfloat16 [4096, 2048], P(('rep', 'fs', 'tp')), may hold values from -6 to 6
- gain_before: float32 [2048], replicated, may hold values from 0.1 to 1.9
- gain_after: float32 [2048], replicated, may hold values from 0.1 to 1.9
- proj_gate: bfloat16 [2048, 3584], P('fs', 'tp'), may hold values from -0.125 to 0.125
- proj_lift: bfloat16 [2048, 3584], P('fs', 'tp'), may hold values from -0.125 to 0.125
- proj_down: bfloat16 [3584, 2048], P('tp', 'fs'), may hold values from -0.09375 to 0.09375
- mixer_gain: float32 [2048], replicated, may hold values from 0.1 to 1.9
- mixer_u: bfloat16 [2048, 2048], P('fs', 'tp'), may hold values from -0.125 to 0.125
- mixer_v: bfloat16 [2048, 2048], P('fs', 'tp'), may hold values from -1 to 1
- layer_gain: float32 [2048], P('tp'), may hold values from 0.1 to 1.9
- layer_shift: float32 [2048], P('tp'), may hold values from -3 to 3
- spatial: bfloat16 [16, 128, 128], P('tp'), may hold values from -0.5 to 0.5
- spatial_shift: float32 [16, 128], P('tp'), may hold values from 0.2 to 2
- mixer_down: bfloat16 [2048, 2048], P('tp', 'fs'), may hold values from -0.125 to 0.125
Outputs:
- result: bfloat16 [4096, 2048], P(('rep', 'fs', 'tp'))
All inputs are finite; a program needn't handle non-finite values.
Results may differ from a plain program's by a relative error of at most 0.017.
Values may be sent and summed in bfloat16 or wider, within the bound.
A program may use at most 128 MiB of HBM per device.

v0:
```python
import jax
import jax.numpy as jnp
from jax import lax
from jax.sharding import PartitionSpec as P

GROUP_DIM = 128
SPAN = 128
A = 2048
norm_epsilon = 1e-06
layer_epsilon = 1e-05


def norm_rows(row_block, scale_gain):
    widened = row_block.astype(jnp.float32)
    factor = lax.rsqrt(jnp.mean(widened * widened, axis=1, keepdims=True) + norm_epsilon)
    return (widened * factor * scale_gain).astype(jnp.bfloat16)


def gathered_norm(stream_rows, scale_gain):
    gathered = lax.all_gather(stream_rows, "tp", axis=0, tiled=True)
    return norm_rows(gathered, scale_gain)


def pair_adder(normed, pieces):
    return (
        jnp.dot(normed, pieces[0], preferred_element_type=jnp.float32),
        jnp.dot(normed, pieces[1], preferred_element_type=jnp.float32),
    )


def activate(gate_vals, lift_vals):
    return (jax.nn.silu(gate_vals) * lift_vals).astype(jnp.bfloat16)


def half_again(stream_rows, scale_gain, proj_gate, proj_lift, proj_down):
    normed = gathered_norm(stream_rows, scale_gain)
    gate_vals, lift_vals = pair_adder(
        normed,
        (
            lax.all_gather(proj_gate, "fs", axis=0, tiled=True),
            lax.all_gather(proj_lift, "fs", axis=0, tiled=True),
        ),
    )
    hidden = activate(gate_vals, lift_vals)
    partial_value = jnp.dot(
        hidden,
        lax.all_gather(proj_down, "fs", axis=1, tiled=True),
        preferred_element_type=jnp.float32,
    )
    summed = lax.psum_scatter(
        partial_value.astype(jnp.bfloat16), "tp", scatter_dimension=0, tiled=True
    ).astype(jnp.float32)
    return (stream_rows.astype(jnp.float32) + 0.5 * summed).astype(jnp.bfloat16)


def token_mixer(
    stream_rows,
    mixer_gain,
    mixer_u,
    mixer_v,
    layer_gain,
    layer_shift,
    spatial,
    spatial_shift,
    mixer_down,
):
    gathered = lax.all_gather(stream_rows, "tp", axis=0, tiled=True)
    normed = norm_rows(gathered, mixer_gain)
    seq_tokens = normed.shape[0]
    u_vals, v_vals = pair_adder(
        normed,
        (
            lax.all_gather(mixer_u, "fs", axis=0, tiled=True),
            lax.all_gather(mixer_v, "fs", axis=0, tiled=True),
        ),
    )
    lifted = jax.nn.gelu(v_vals)
    moments = lax.psum((jnp.sum(lifted, axis=1), jnp.sum(lifted * lifted, axis=1)), "tp")
    centre = moments[0] / A
    spread = moments[1] / A - centre * centre
    normed_v = (
        (lifted - centre[:, None]) * lax.rsqrt(spread[:, None] + layer_epsilon) * layer_gain
        + layer_shift
    ).astype(jnp.bfloat16)
    groups_here = spatial.shape[0]
    blocked = normed_v.reshape(seq_tokens // SPAN, SPAN, groups_here, GROUP_DIM)
    causal = jnp.tril(jnp.ones((SPAN, SPAN), dtype=bool))
    masked = jnp.where(causal[None], spatial, jnp.zeros((), jnp.bfloat16))
    mixed_v = jnp.einsum("gts,bsgd->btgd", masked, blocked, preferred_element_type=jnp.float32)
    mixed_v = mixed_v + spatial_shift.T[None, :, :, None]
    gated = (jax.nn.gelu(u_vals) * mixed_v.reshape(seq_tokens, groups_here * GROUP_DIM)).astype(
        jnp.bfloat16
    )
    partial_value = jnp.dot(
        gated,
        lax.all_gather(mixer_down, "fs", axis=1, tiled=True),
        preferred_element_type=jnp.float32,
    )
    summed = lax.psum_scatter(
        partial_value.astype(jnp.bfloat16), "tp", scatter_dimension=0, tiled=True
    ).astype(jnp.float32)
    return (stream_rows.astype(jnp.float32) + summed).astype(jnp.bfloat16)


def body(
    stream,
    gain_before,
    gain_after,
    proj_gate,
    proj_lift,
    proj_down,
    mixer_gain,
    mixer_u,
    mixer_v,
    layer_gain,
    layer_shift,
    spatial,
    spatial_shift,
    mixer_down,
):
    first = half_again(stream, gain_before, proj_gate, proj_lift, proj_down)
    second = token_mixer(
        first,
        mixer_gain,
        mixer_u,
        mixer_v,
        layer_gain,
        layer_shift,
        spatial,
        spatial_shift,
        mixer_down,
    )
    result = half_again(second, gain_after, proj_gate, proj_lift, proj_down)
    return result


def solution(mesh):
    placed = (
        P(("rep", "fs", "tp"), None),
        P(),
        P(),
        P("fs", "tp"),
        P("fs", "tp"),
        P("tp", "fs"),
        P(),
        P("fs", "tp"),
        P("fs", "tp"),
        P("tp"),
        P("tp"),
        P("tp", None, None),
        P("tp", None),
        P("tp", "fs"),
    )
    return jax.shard_map(
        body, mesh=mesh, in_specs=placed, out_specs=P(("rep", "fs", "tp"), None), check_vma=False
    )
```

profile of v0, /device:TPU:0, one launch (start us, length us, event | category | flops | bytes accessed | tf_op | source)
XLA Modules:
  0.0 575.2 jit_solution(15976335767558670113)
XLA Ops:
  6.5 0.7 all-gather.10.cloned.1.call-update
  7.3 0.7 all-gather.12.cloned.1.call-update
  9.4 24.8 %all-gather.10.cloned.1.call-done = bf16[512,2048]{1,0:T(8,128)(2,1)} async-done(((bf16[128,2048]{1,0:T(8,128)(2,1)}), bf16[512,2048]{1,0:T(8,128)(2,1)}) %all-gather.10.cloned.1.call-update) | async-done | bytes 2097168 | tf_op jit(solution)/shard_map/all_gather | solution.py:20
  34.2 2.2 fusion
  36.4 71.5 %all-gather.12.cloned.1.call-done = bf16[2048,896]{1,0:T(8,128)(2,1)} async-done(((bf16[512,896]{1,0:T(8,128)(2,1)}), bf16[2048,896]{1,0:T(8,128)(2,1)}) %all-gather.12.cloned.1.call-update) | async-done | bytes 3670032 | tf_op jit(solution)/shard_map/all_gather | solution.py:40
  107.9 5.6 fusion.42
  113.5 66.6 %all-gather.14.cloned.1.call-done = bf16[2048,896]{1,0:T(8,128)(2,1)} async-done(((bf16[512,896]{1,0:T(8,128)(2,1)}), bf16[2048,896]{1,0:T(8,128)(2,1)}) %all-gather.14.cloned.1.call-update) | async-done | bytes 3670032 | tf_op jit(solution)/shard_map/all_gather | solution.py:41
  180.2 72.1 %all-gather.16.cloned.1.call-done = bf16[896,2048]{1,0:T(8,128)(2,1)} async-done(((bf16[896,512]{1,0:T(8,128)(2,1)}), bf16[896,2048]{1,0:T(8,128)(2,1)}) %all-gather.16.cloned.1.call-update) | async-done | bytes 3670032 | tf_op jit(solution)/shard_map/all_gather | solution.py:47
  252.3 9.7 %convolution_convert_fusion.1 = bf16[512,2048]{1,0:T(8,128)(2,1)} fusion(bf16[896,2048]{1,0:T(8,128)(2,1)} %all-gather.16.cloned.1.call-done, f32[512,896]{1,0:T(8,128)} %fusion.42, bf16[2048,896]{1,0:T(8,128)(2,1)} %all-gather.14.cloned.1.call-done, bf16[512,2048]{1,0:T(8,128)(2,1)S(1)} %copy-done.4, f32[2048]{0:T(1024)S(1)} %copy-done.10, ...), kind=kOutput, calls=%fused_computation.16 | convolution fusion | flops 3766091776 | bytes 13379584 | tf_op jit(solution)/shard_map/dot_general | solution.py:45
  262.0 29.9 %reduce-scatter.4.cloned.1.call-done = bf16[128,2048]{1,0:T(8,128)(2,1)} async-done(((bf16[512,2048]{1,0:T(8,128)(2,1)}), bf16[128,2048]{1,0:T(8,128)(2,1)}) %reduce-scatter.4.cloned.1.call-update) | async-done | bytes 524304 | tf_op jit(solution)/shard_map/reduce_scatter | solution.py:50
  291.9 2.0 add_convert_fusion.3
  294.0 0.7 all-gather.22.cloned.1.call-update
  296.2 20.4 %all-gather.18.cloned.1.call-done = bf16[512,2048]{1,0:T(8,128)(2,1)} async-done(((bf16[128,2048]{1,0:T(8,128)(2,1)}), bf16[512,2048]{1,0:T(8,128)(2,1)}) %all-gather.18.cloned.1.call-update) | async-done | bytes 2097168 | tf_op jit(solution)/shard_map/all_gather | solution.py:67
  316.6 2.2 fusion.3
  318.9 45.0 %all-gather.22.cloned.1.call-done = bf16[2048,512]{1,0:T(8,128)(2,1)} async-done(((bf16[512,512]{1,0:T(8,128)(2,1)}), bf16[2048,512]{1,0:T(8,128)(2,1)}) %all-gather.22.cloned.1.call-update) | async-done | bytes 2097168 | tf_op jit(solution)/shard_map/all_gather | solution.py:74
  363.9 4.1 fusion.60
  368.0 6.5 %all-reduce = (f32[512]{0:T(512)S(1)}, f32[512]{0:T(512)S(1)}) all-reduce(f32[512]{0:T(512)S(1)} %get-tuple-element.6, f32[512]{0:T(512)S(1)} %get-tuple-element.5), channel_id=1, replica_groups=mesh['rep'=2,'fs'=4,'tp'=4] {'tp'}, use_global_device_ids=true, to_apply=%region_6.7 | all-reduce | flops 1024 | bytes 8192 | tf_op jit(solution)/shard_map/psum | solution.py:78
  374.6 1.5 add_convert_fusion.2
  376.0 0.9 reshape.47
  377.0 1.4 fusion.9
  378.4 1.3 copy.21
  379.7 30.2 %all-gather.20.cloned.1.call-done = bf16[2048,512]{1,0:T(8,128)(2,1)} async-done(((bf16[512,512]{1,0:T(8,128)(2,1)}), bf16[2048,512]{1,0:T(8,128)(2,1)}) %all-gather.20.cloned.1.call-update) | async-done | bytes 2097168 | tf_op jit(solution)/shard_map/all_gather | solution.py:73
  409.9 46.1 %all-gather.24.cloned.1.call-done = bf16[512,2048]{1,0:T(8,128)(2,1)} async-done(((bf16[512,512]{1,0:T(8,128)(2,1)}), bf16[512,2048]{1,0:T(8,128)(2,1)}) %all-gather.24.cloned.1.call-update) | async-done | bytes 2097168 | tf_op jit(solution)/shard_map/all_gather | solution.py:96
  456.0 6.5 %convolution_convert_fusion.2 = bf16[512,2048]{1,0:T(8,128)(2,1)} fusion(bf16[512,2048]{1,0:T(8,128)(2,1)} %all-gather.24.cloned.1.call-done, f32[64,8,4,128]{3,2,1,0:T(4,128)} %bitcast.25, bf16[2048,512]{1,0:T(8,128)(2,1)} %all-gather.20.cloned.1.call-done, bf16[512,2048]{1,0:T(8,128)(2,1)S(1)} %copy-done.3, f32[2048]{0:T(1024)S(1)} %copy-done.11, ...), kind=kOutput, calls=%fused_computation.17 | convolution fusion | flops 2155347968 | bytes 9447424 | tf_op jit(solution)/shard_map/dot_general | solution.py:94
  462.6 30.1 %reduce-scatter.6.cloned.1.call-done = bf16[128,2048]{1,0:T(8,128)(2,1)} async-done(((bf16[512,2048]{1,0:T(8,128)(2,1)}), bf16[128,2048]{1,0:T(8,128)(2,1)}) %reduce-scatter.6.cloned.1.call-update) | async-done | bytes 524304 | tf_op jit(solution)/shard_map/reduce_scatter | solution.py:99
  492.7 2.0 add_convert_fusion.1
  494.9 22.5 %all-gather.26.cloned.1.call-done = bf16[512,2048]{1,0:T(8,128)(2,1)} async-done(((bf16[128,2048]{1,0:T(8,128)(2,1)}), bf16[512,2048]{1,0:T(8,128)(2,1)}) %all-gather.26.cloned.1.call-update) | async-done | bytes 2097168 | tf_op jit(solution)/shard_map/all_gather | solution.py:20
  517.4 2.2 fusion.6
  519.6 5.7 fusion.28
  525.3 9.7 %convolution_convert_fusion = bf16[512,2048]{1,0:T(8,128)(2,1)} fusion(bf16[896,2048]{1,0:T(8,128)(2,1)} %all-gather.16.cloned.1.call-done, f32[512,896]{1,0:T(8,128)} %fusion.28, bf16[2048,896]{1,0:T(8,128)(2,1)} %all-gather.14.cloned.1.call-done, bf16[512,2048]{1,0:T(8,128)(2,1)S(1)} %copy-done.5, f32[2048]{0:T(1024)S(1)} %copy-done.12, ...), kind=kOutput, calls=%fused_computation.15 | convolution fusion | flops 3766091776 | bytes 13379584 | tf_op jit(solution)/shard_map/dot_general | solution.py:45
  535.0 31.3 %reduce-scatter.8.cloned.1.call-done = bf16[128,2048]{1,0:T(8,128)(2,1)} async-done(((bf16[512,2048]{1,0:T(8,128)(2,1)}), bf16[128,2048]{1,0:T(8,128)(2,1)}) %reduce-scatter.8.cloned.1.call-update) | async-done | bytes 524304 | tf_op jit(solution)/shard_map/reduce_scatter | solution.py:50
  566.4 2.0 add_convert_fusion
  (52 shorter events, 3.4 us)
Async XLA Ops:
  6.5 27.7 %all-gather.10.cloned.1.call-start = ((), (), s32[]{:S(2)}) async-start(), calls=%async_computation.3 | async-start | bytes 2621440 | tf_op jit(solution)/shard_map/all_gather | solution.py:20
  7.3 100.6 %all-gather.12.cloned.1.call-start = ((), (), s32[]{:S(2)}) async-start(), calls=%async_computation.4 | async-start | bytes 4587520 | tf_op jit(solution)/shard_map/all_gather | solution.py:40
  8.0 99.9 %copy-start.10 = (f32[2048]{0:T(1024)S(1)}, f32[2048]{0:T(1024)}, u32[]{:S(2)}) copy-start(f32[2048]{0:T(1024)} %param.15) | copy-start | bytes 24580
  8.0 172.2 %all-gather.14.cloned.1.call-start = ((), (), s32[]{:S(2)}) async-start(), calls=%async_computation.5 | async-start | bytes 4587520 | tf_op jit(solution)/shard_map/all_gather | solution.py:41
  8.8 243.5 %all-gather.16.cloned.1.call-start = ((), (), s32[]{:S(2)}) async-start(), calls=%async_computation.6 | async-start | bytes 4587520 | tf_op jit(solution)/shard_map/all_gather | solution.py:47
  9.3 282.6 %reduce-scatter.4.cloned.1.call-start = ((), (), s32[]{:S(2)}) async-start(), calls=%async_computation.7 | async-start | bytes 2621440 | tf_op jit(solution)/shard_map/reduce_scatter | solution.py:50
  34.2 73.7 %copy-start.4 = (bf16[512,2048]{1,0:T(8,128)(2,1)S(1)}, bf16[512,2048]{1,0:T(8,128)(2,1)}, u32[]{:S(2)}) copy-start(bf16[512,2048]{1,0:T(8,128)(2,1)} %all-gather.10.cloned.1.call-done) | copy-start | bytes 6291460
  262.0 29.9 %copy-start.2 = (bf16[128,2048]{1,0:T(8,128)(2,1)S(1)}, bf16[128,2048]{1,0:T(8,128)(2,1)}, u32[]{:S(2)}) copy-start(bf16[128,2048]{1,0:T(8,128)(2,1)} %param.14) | copy-start | bytes 1572868
  262.0 54.6 %all-gather.18.cloned.1.call-start = ((), (), s32[]{:S(2)}) async-start(), calls=%async_computation.8 | async-start | bytes 2621440 | tf_op jit(solution)/shard_map/all_gather | solution.py:67
  293.9 70.0 %copy-start.11 = (f32[2048]{0:T(1024)S(1)}, f32[2048]{0:T(1024)}, u32[]{:S(2)}) copy-start(f32[2048]{0:T(1024)} %param.20) | copy-start | bytes 24580
  293.9 70.0 %all-gather.22.cloned.1.call-start = ((), (), s32[]{:S(2)}) async-start(), calls=%async_computation.10 | async-start | bytes 2621440 | tf_op jit(solution)/shard_map/all_gather | solution.py:74
  294.7 115.3 %all-gather.20.cloned.1.call-start = ((), (), s32[]{:S(2)}) async-start(), calls=%async_computation.9 | async-start | bytes 2621440 | tf_op jit(solution)/shard_map/all_gather | solution.py:73
  295.4 160.6 %all-gather.24.cloned.1.call-start = ((), (), s32[]{:S(2)}) async-start(), calls=%async_computation.11 | async-start | bytes 2621440 | tf_op jit(solution)/shard_map/all_gather | solution.py:96
  296.2 196.5 %reduce-scatter.6.cloned.1.call-start = ((), (), s32[]{:S(2)}) async-start(), calls=%async_computation.12 | async-start | bytes 2621440 | tf_op jit(solution)/shard_map/reduce_scatter | solution.py:99
  316.6 47.3 %copy-start.3 = (bf16[512,2048]{1,0:T(8,128)(2,1)S(1)}, bf16[512,2048]{1,0:T(8,128)(2,1)}, u32[]{:S(2)}) copy-start(bf16[512,2048]{1,0:T(8,128)(2,1)} %all-gather.18.cloned.1.call-done) | copy-start | bytes 6291460
  318.9 55.7 %copy-start.7 = (f32[512]{0:T(512)S(1)}, f32[512]{0:T(512)}, u32[]{:S(2)}) copy-start(f32[512]{0:T(512)} %param.24) | copy-start | bytes 6148
  318.9 55.7 %copy-start.8 = (f32[512]{0:T(512)S(1)}, f32[512]{0:T(512)}, u32[]{:S(2)}) copy-start(f32[512]{0:T(512)} %param.23) | copy-start | bytes 6148
  368.0 8.9 %copy-start.6 = (bf16[4,128,128]{2,1,0:T(8,128)(2,1)S(1)}, bf16[4,128,128]{2,1,0:T(8,128)(2,1)}, u32[]{:S(2)}) copy-start(bf16[4,128,128]{2,1,0:T(8,128)(2,1)} %param.25) | copy-start | bytes 393220
  368.0 8.9 %copy-start.9 = (f32[4,128]{1,0:T(4,128)S(1)}, f32[4,128]{1,0:T(4,128)}, u32[]{:S(2)}) copy-start(f32[4,128]{1,0:T(4,128)} %param.26) | copy-start | bytes 6148
  462.5 30.2 %copy-start = (bf16[128,2048]{1,0:T(8,128)(2,1)S(1)}, bf16[128,2048]{1,0:T(8,128)(2,1)}, u32[]{:S(2)}) copy-start(bf16[128,2048]{1,0:T(8,128)(2,1)} %add_convert_fusion.3) | copy-start | bytes 1572868
  462.5 57.1 %copy-start.12 = (f32[2048]{0:T(1024)S(1)}, f32[2048]{0:T(1024)}, u32[]{:S(2)}) copy-start(f32[2048]{0:T(1024)} %param.16) | copy-start | bytes 24580
  462.5 54.8 %all-gather.26.cloned.1.call-start = ((), (), s32[]{:S(2)}) async-start(), calls=%async_computation.13 | async-start | bytes 2621440 | tf_op jit(solution)/shard_map/all_gather | solution.py:20
  494.6 71.7 %reduce-scatter.8.cloned.1.call-start = ((), (), s32[]{:S(2)}) async-start(), calls=%async_computation.14 | async-start | bytes 2621440 | tf_op jit(solution)/shard_map/reduce_scatter | solution.py:50
  517.4 2.2 copy-start.5
  535.0 31.4 %copy-start.1 = (bf16[128,2048]{1,0:T(8,128)(2,1)S(1)}, bf16[128,2048]{1,0:T(8,128)(2,1)}, u32[]{:S(2)}) copy-start(bf16[128,2048]{1,0:T(8,128)(2,1)} %add_convert_fusion.1) | copy-start | bytes 1572868
Sparse Core Ops, SparseCore 0:
  8.9 25.2 all-gather.9
  35.8 72.0 all-gather.11
  109.5 70.6 all-gather.13
  181.6 70.6 all-gather.15
  262.1 29.7 reduce-scatter.3
  294.1 22.5 all-gather.17
  318.2 45.6 all-gather.21
  365.5 44.4 all-gather.19
  411.5 44.4 all-gather.23
  462.6 29.9 reduce-scatter.5
  494.8 22.5 all-gather.25
  535.1 31.1 reduce-scatter.7
where the time goes:
time: 576 us; the launch traced here: 575 us
  waiting for transfers between devices  495 us (86%)
  matrix products  42.7 us (7%)
  other arithmetic  14.1 us (2%)
  between operations  13.7 us (2%)
  blocking collectives  6.51 us (1%)
    all_gather x1, waiting for transfers between devices, half_again(): lax.all_gather(proj_down, 'fs', axis=1, tiled=True)  72.1 us
    all_gather x1, waiting for transfers between devices, half_again(): lax.all_gather(proj_gate, 'fs', axis=0, tiled=True)  71.5 us
    all_gather x1, waiting for transfers between devices, half_again(): lax.all_gather(proj_lift, 'fs', axis=0, tiled=True)  66.6 us
    reduce_scatter x2, waiting for transfers between devices, half_again(): lax.psum_scatter(partial_value.astype(jnp.bfloat16), 'tp', scatter_dimens...  61.2 us
    all_gather x2, waiting for transfers between devices, gathered_norm(): gathered = lax.all_gather(stream_rows, 'tp', axis=0, tiled=True)  47.3 us
    all_gather x1, waiting for transfers between devices, token_mixer(): lax.all_gather(mixer_down, 'fs', axis=1, tiled=True)  46.1 us
    all_gather x1, waiting for transfers between devices, token_mixer(): lax.all_gather(mixer_v, 'fs', axis=0, tiled=True)  45 us
    all_gather x1, waiting for transfers between devices, token_mixer(): lax.all_gather(mixer_u, 'fs', axis=0, tiled=True)  30.2 us
  transfers between devices with their start and end apart: 12, of which 12 were waited for; matrix products, arithmetic and copies ran while one was open for 3% of the time, Pallas kernels for 0%

commit v1 on v0

--- a/solution.py
+++ b/solution.py
@@ -8,6 +8,40 @@
 A = 2048
 norm_epsilon = 1e-06
 layer_epsilon = 1e-05
+
+
+def samples_deliver(in_array, axis_id):
+    current_arr, a_next, inter = (
+        jax.lax.axis_size(axis_id),
+        jax.lax.axis_index(axis_id),
+        in_array.shape[0],
+    )
+    copies = [
+        src_i * current_arr if to_i == 0 else src_i for to_i, src_i in enumerate(in_array.shape)
+    ]
+    mat_out = lax.dynamic_update_slice_in_dim(
+        jnp.zeros(copies, in_array.dtype), in_array, a_next * inter, axis=0
+    )
+    n_now = arr_next = in_array
+    for tick in range(1, current_arr // 2 + 1):
+        n_now = jax.lax.ppermute(
+            n_now,
+            axis_name=axis_id,
+            perm=list(map(lambda to_i: (to_i, (to_i + 1) % current_arr), range(current_arr))),
+        )
+        mat_out = lax.dynamic_update_slice_in_dim(
+            mat_out, n_now, (a_next - tick) % current_arr * inter, axis=0
+        )
+        if 2 * tick < current_arr:
+            arr_next = jax.lax.ppermute(
+                arr_next,
+                axis_id,
+                perm=list(map(lambda to_i: (to_i, (to_i - 1) % current_arr), range(current_arr))),
+            )
+            mat_out = lax.dynamic_update_slice_in_dim(
+                mat_out, arr_next, (a_next + tick) % current_arr * inter, axis=0
+            )
+    return mat_out
 
 
 def norm_rows(row_block, scale_gain):
@@ -36,10 +70,7 @@
     normed = gathered_norm(stream_rows, scale_gain)
     gate_vals, lift_vals = pair_adder(
         normed,
-        (
-            lax.all_gather(proj_gate, "fs", axis=0, tiled=True),
-            lax.all_gather(proj_lift, "fs", axis=0, tiled=True),
-        ),
+        (lax.all_gather(proj_gate, "fs", axis=0, tiled=True), samples_deliver(proj_lift, "fs")),
     )
     hidden = activate(gate_vals, lift_vals)
     partial_value = jnp.dot(

time: 576 us -> 529 us (0.918)
  waiting for transfers between devices: 495 us -> 436 us
  local copies, waits for them, and re-layouts: 2.34 us -> 9.91 us
    ppermute x0 -> x3, waiting for transfers between devices: none -> 79.1 us  [the longest x2 45.6 us: samples_deliver(): jax.lax.ppermute(n_now, axis_name=axis_id, perm=list(map(lambda to_i: (to...]
    all_gather x1 -> x0, waiting for transfers between devices: 66.6 us -> none  [half_again(): lax.all_gather(proj_lift, 'fs', axis=0, tiled=True)]
    all_gather x1, waiting for transfers between devices: 71.5 us -> 30.3 us  [half_again(): lax.all_gather(proj_gate, 'fs', axis=0, tiled=True)]
    all_gather x2, waiting for transfers between devices: 47.3 us -> 22.7 us  [gathered_norm(): gathered = lax.all_gather(stream_rows, 'tp', axis=0, tiled=True)]
  transfers between devices with their start and end apart: 12 -> 14, of which waited for: 12 -> 13; matrix products, arithmetic and copies ran while one was open for 3% -> 5% of each run, Pallas kernels for 0% -> 0%
where the time goes in v1:
time: 529 us; the launch traced here: 528 us
  waiting for transfers between devices  436 us (82%)
  matrix products  42.7 us (8%)
  other arithmetic  14.1 us (3%)
  between operations  13.3 us (3%)
  local copies, waits for them, and re-layouts  9.91 us (2%)
  blocking collectives  6.69 us (1%)
  starting transfers between devices  5.6 us (1%)
    all_gather x1, waiting for transfers between devices, half_again(): lax.all_gather(proj_down, 'fs', axis=1, tiled=True)  67.2 us
    reduce_scatter x2, waiting for transfers between devices, half_again(): lax.psum_scatter(partial_value.astype(jnp.bfloat16), 'tp', scatter_dimens...  61.2 us
    all_gather x1, waiting for transfers between devices, token_mixer(): lax.all_gather(mixer_down, 'fs', axis=1, tiled=True)  46.1 us
    ppermute x2, waiting for transfers between devices, samples_deliver(): jax.lax.ppermute(n_now, axis_name=axis_id, perm=list(map(lambda to_i: (to...  45.6 us
    all_gather x1, waiting for transfers between devices, token_mixer(): lax.all_gather(mixer_v, 'fs', axis=0, tiled=True)  44.9 us
    ppermute x1, waiting for transfers between devices, samples_deliver(): jax.lax.ppermute(arr_next, axis_id, perm=list(map(lambda to_i: (to_i, (to...  33.4 us
    all_gather x1, waiting for transfers between devices, half_again(): lax.all_gather(proj_gate, 'fs', axis=0, tiled=True)  30.3 us
    reduce_scatter x1, waiting for transfers between devices, token_mixer(): lax.psum_scatter(partial_value.astype(jnp.bfloat16), 'tp', scatter_dimens...  30.1 us
  transfers between devices with their start and end apart: 14, of which 13 were waited for; matrix products, arithmetic and copies ran while one was open for 5% of the time, Pallas kernels for 0%

profile of v1, /device:TPU:0, one launch (start us, length us, event | category | flops | bytes accessed | tf_op | source)
XLA Modules:
  0.0 528.4 jit_solution(1927523975750392994)
XLA Ops:
  8.8 3.1 collective-permute-start
  11.9 2.1 collective-permute-start.1
  14.0 21.2 %collective-permute-done = bf16[512,896]{1,0:T(8,128)(2,1)S(1)} collective-permute-done((bf16[512,896]{1,0:T(8,128)(2,1)S(1)}, bf16[512,896]{1,0:T(8,128)(2,1)S(1)}, u32[]{:S(2)}, u32[]{:S(2)}) %collective-permute-start) | collective-permute-done | bytes 917536 | tf_op jit(solution)/shard_map/ppermute | solution.py:27
  35.2 2.2 broadcast.77
  39.5 33.4 %collective-permute-done.1 = bf16[512,896]{1,0:T(8,128)(2,1)} collective-permute-done((bf16[512,896]{1,0:T(8,128)(2,1)S(1)}, bf16[512,896]{1,0:T(8,128)(2,1)}, u32[]{:S(2)}, u32[]{:S(2)}) %collective-permute-start.1) | collective-permute-done | bytes 917536 | tf_op jit(solution)/shard_map/ppermute | solution.py:36
  72.9 2.3 constant_dynamic-update-slice_fusion.1
  75.2 24.5 %collective-permute-done.2 = bf16[512,896]{1,0:T(8,128)(2,1)S(1)} collective-permute-done((bf16[512,896]{1,0:T(8,128)(2,1)S(1)}, bf16[512,896]{1,0:T(8,128)(2,1)S(1)}, u32[]{:S(2)}, u32[]{:S(2)}) %collective-permute-start.2) | collective-permute-done | bytes 917536 | tf_op jit(solution)/shard_map/ppermute | solution.py:27
  100.6 2.2 fusion
  102.9 30.3 %all-gather.11.cloned.1.call-done = bf16[2048,896]{1,0:T(8,128)(2,1)} async-done(((bf16[512,896]{1,0:T(8,128)(2,1)}), bf16[2048,896]{1,0:T(8,128)(2,1)}) %all-gather.11.cloned.1.call-update) | async-done | bytes 3670032 | tf_op jit(solution)/shard_map/all_gather | solution.py:73
  133.2 5.6 %fusion.42 = f32[512,896]{1,0:T(8,128)} fusion(bf16[2048,896]{1,0:T(8,128)(2,1)} %all-gather.11.cloned.1.call-done, bf16[512,2048]{1,0:T(8,128)(2,1)S(1)} %copy-done.3, f32[2048]{0:T(1024)S(1)} %copy-done.11, f32[512]{0:T(512)S(1)} %add_rsqrt_fusion.3), kind=kOutput, calls=%fused_computation.48 | convolution fusion | flops 1883242496 | bytes 7612416 | tf_op jit(solution)/shard_map/dot_general | solution.py:60
  138.8 67.2 %all-gather.13.cloned.1.call-done = bf16[896,2048]{1,0:T(8,128)(2,1)} async-done(((bf16[896,512]{1,0:T(8,128)(2,1)}), bf16[896,2048]{1,0:T(8,128)(2,1)}) %all-gather.13.cloned.1.call-update) | async-done | bytes 3670032 | tf_op jit(solution)/shard_map/all_gather | solution.py:78
  206.0 9.7 %convolution_convert_fusion.1 = bf16[512,2048]{1,0:T(8,128)(2,1)} fusion(bf16[896,2048]{1,0:T(8,128)(2,1)} %all-gather.13.cloned.1.call-done, f32[512,896]{1,0:T(8,128)} %fusion.42, bf16[2048,896]{1,0:T(8,128)(2,1)} %constant_dynamic-update-slice_fusion, bf16[512,2048]{1,0:T(8,128)(2,1)S(1)} %copy-done.3, f32[2048]{0:T(1024)S(1)} %copy-done.11, ...), kind=kOutput, calls=%fused_computation.16 | convolution fusion | flops 3766091776 | bytes 13379584 | tf_op jit(solution)/shard_map/dot_general | solution.py:76
  215.8 29.8 %reduce-scatter.4.cloned.1.call-done = bf16[128,2048]{1,0:T(8,128)(2,1)} async-done(((bf16[512,2048]{1,0:T(8,128)(2,1)}), bf16[128,2048]{1,0:T(8,128)(2,1)}) %reduce-scatter.4.cloned.1.call-update) | async-done | bytes 524304 | tf_op jit(solution)/shard_map/reduce_scatter | solution.py:81
  245.6 2.0 add_convert_fusion.3
  249.8 20.6 %all-gather.15.cloned.1.call-done = bf16[512,2048]{1,0:T(8,128)(2,1)} async-done(((bf16[128,2048]{1,0:T(8,128)(2,1)}), bf16[512,2048]{1,0:T(8,128)(2,1)}) %all-gather.15.cloned.1.call-update) | async-done | bytes 2097168 | tf_op jit(solution)/shard_map/all_gather | solution.py:98
  270.3 2.2 fusion.3
  272.6 44.9 %all-gather.19.cloned.1.call-done = bf16[2048,512]{1,0:T(8,128)(2,1)} async-done(((bf16[512,512]{1,0:T(8,128)(2,1)}), bf16[2048,512]{1,0:T(8,128)(2,1)}) %all-gather.19.cloned.1.call-update) | async-done | bytes 2097168 | tf_op jit(solution)/shard_map/all_gather | solution.py:105
  317.5 4.2 fusion.60
  321.6 6.7 %all-reduce = (f32[512]{0:T(512)S(1)}, f32[512]{0:T(512)S(1)}) all-reduce(f32[512]{0:T(512)S(1)} %get-tuple-element.6, f32[512]{0:T(512)S(1)} %get-tuple-element.5), channel_id=1, replica_groups=mesh['rep'=2,'fs'=4,'tp'=4] {'tp'}, use_global_device_ids=true, to_apply=%region_6.7 | all-reduce | flops 1024 | bytes 8192 | tf_op jit(solution)/shard_map/psum | solution.py:109
  328.3 1.5 add_convert_fusion.2
  330.7 1.4 fusion.9
  333.5 30.0 %all-gather.17.cloned.1.call-done = bf16[2048,512]{1,0:T(8,128)(2,1)} async-done(((bf16[512,512]{1,0:T(8,128)(2,1)}), bf16[2048,512]{1,0:T(8,128)(2,1)}) %all-gather.17.cloned.1.call-update) | async-done | bytes 2097168 | tf_op jit(solution)/shard_map/all_gather | solution.py:104
  363.5 46.1 %all-gather.21.cloned.1.call-done = bf16[512,2048]{1,0:T(8,128)(2,1)} async-done(((bf16[512,512]{1,0:T(8,128)(2,1)}), bf16[512,2048]{1,0:T(8,128)(2,1)}) %all-gather.21.cloned.1.call-update) | async-done | bytes 2097168 | tf_op jit(solution)/shard_map/all_gather | solution.py:127
  409.6 6.5 %convolution_convert_fusion.2 = bf16[512,2048]{1,0:T(8,128)(2,1)} fusion(bf16[512,2048]{1,0:T(8,128)(2,1)} %all-gather.21.cloned.1.call-done, f32[64,8,4,128]{3,2,1,0:T(4,128)} %bitcast.25, bf16[2048,512]{1,0:T(8,128)(2,1)} %all-gather.17.cloned.1.call-done, bf16[512,2048]{1,0:T(8,128)(2,1)S(1)} %copy-done.4, f32[2048]{0:T(1024)S(1)} %copy-done.12, ...), kind=kOutput, calls=%fused_computation.17 | convolution fusion | flops 2155347968 | bytes 9447424 | tf_op jit(solution)/shard_map/dot_general | solution.py:125
  416.1 30.1 %reduce-scatter.6.cloned.1.call-done = bf16[128,2048]{1,0:T(8,128)(2,1)} async-done(((bf16[512,2048]{1,0:T(8,128)(2,1)}), bf16[128,2048]{1,0:T(8,128)(2,1)}) %reduce-scatter.6.cloned.1.call-update) | async-done | bytes 524304 | tf_op jit(solution)/shard_map/reduce_scatter | solution.py:130
  446.2 2.0 add_convert_fusion.1
  448.3 22.7 %all-gather.23.cloned.1.call-done = bf16[512,2048]{1,0:T(8,128)(2,1)} async-done(((bf16[128,2048]{1,0:T(8,128)(2,1)}), bf16[512,2048]{1,0:T(8,128)(2,1)}) %all-gather.23.cloned.1.call-update) | async-done | bytes 2097168 | tf_op jit(solution)/shard_map/all_gather | solution.py:54
  470.9 2.2 fusion.6
  473.2 5.7 %fusion.28 = f32[512,896]{1,0:T(8,128)} fusion(bf16[2048,896]{1,0:T(8,128)(2,1)} %all-gather.11.cloned.1.call-done, bf16[512,2048]{1,0:T(8,128)(2,1)S(1)} %copy-done.5, f32[2048]{0:T(1024)S(1)} %copy-done.13, f32[512]{0:T(512)S(1)} %add_rsqrt_fusion), kind=kOutput, calls=%fused_computation.45 | convolution fusion | flops 1883242496 | bytes 7612416 | tf_op jit(solution)/shard_map/dot_general | solution.py:60
  478.9 9.6 %convolution_convert_fusion = bf16[512,2048]{1,0:T(8,128)(2,1)} fusion(bf16[896,2048]{1,0:T(8,128)(2,1)} %all-gather.13.cloned.1.call-done, f32[512,896]{1,0:T(8,128)} %fusion.28, bf16[2048,896]{1,0:T(8,128)(2,1)} %constant_dynamic-update-slice_fusion, bf16[512,2048]{1,0:T(8,128)(2,1)S(1)} %copy-done.5, f32[2048]{0:T(1024)S(1)} %copy-done.13, ...), kind=kOutput, calls=%fused_computation.15 | convolution fusion | flops 3766091776 | bytes 13379584 | tf_op jit(solution)/shard_map/dot_general | solution.py:76
  488.5 31.3 %reduce-scatter.8.cloned.1.call-done = bf16[128,2048]{1,0:T(8,128)(2,1)} async-done(((bf16[512,2048]{1,0:T(8,128)(2,1)}), bf16[128,2048]{1,0:T(8,128)(2,1)}) %reduce-scatter.8.cloned.1.call-update) | async-done | bytes 524304 | tf_op jit(solution)/shard_map/reduce_scatter | solution.py:81
  519.9 2.0 add_convert_fusion
  (62 shorter events, 10.0 us)
Async XLA Ops:
  6.5 2.3 copy-start.6
  6.5 94.1 %all-gather.9.cloned.1.call-start = ((), (), s32[]{:S(2)}) async-start(), calls=%async_computation.3 | async-start | bytes 2621440 | tf_op jit(solution)/shard_map/all_gather | solution.py:54
  7.3 125.9 %all-gather.11.cloned.1.call-start = ((), (), s32[]{:S(2)}) async-start(), calls=%async_computation.4 | async-start | bytes 4587520 | tf_op jit(solution)/shard_map/all_gather | solution.py:73
  8.0 198.0 %all-gather.13.cloned.1.call-start = ((), (), s32[]{:S(2)}) async-start(), calls=%async_computation.5 | async-start | bytes 4587520 | tf_op jit(solution)/shard_map/all_gather | solution.py:78
  8.7 236.8 %reduce-scatter.4.cloned.1.call-start = ((), (), s32[]{:S(2)}) async-start(), calls=%async_computation.6 | async-start | bytes 2621440 | tf_op jit(solution)/shard_map/reduce_scatter | solution.py:81
  8.8 26.4 %collective-permute-start = (bf16[512,896]{1,0:T(8,128)(2,1)S(1)}, bf16[512,896]{1,0:T(8,128)(2,1)S(1)}, u32[]{:S(2)}, u32[]{:S(2)}) collective-permute-start(bf16[512,896]{1,0:T(8,128)(2,1)S(1)} %copy-done.6), channel_id=1, source_target_pairs={{0,4},{4,8},{8,12},{12,0},{1,5},{5,9},{9,13},{13,1},{2,6},{6,10},{... | collective-permute-start | bytes 2752520 | tf_op jit(solution)/shard_map/ppermute | solution.py:27
  11.9 61.0 %collective-permute-start.1 = (bf16[512,896]{1,0:T(8,128)(2,1)S(1)}, bf16[512,896]{1,0:T(8,128)(2,1)}, u32[]{:S(2)}, u32[]{:S(2)}) collective-permute-start(bf16[512,896]{1,0:T(8,128)(2,1)S(1)} %copy-done.6), channel_id=1, source_target_pairs={{0,12},{4,0},{8,4},{12,8},{1,13},{5,1},{9,5},{13,9},{2,14},{6,2},{... | collective-permute-start | bytes 2752520 | tf_op jit(solution)/shard_map/ppermute | solution.py:36
  35.2 64.4 %collective-permute-start.2 = (bf16[512,896]{1,0:T(8,128)(2,1)S(1)}, bf16[512,896]{1,0:T(8,128)(2,1)S(1)}, u32[]{:S(2)}, u32[]{:S(2)}) collective-permute-start(bf16[512,896]{1,0:T(8,128)(2,1)S(1)} %collective-permute-done), channel_id=1, source_target_pairs={{0,4},{4,8},{8,12},{12,0},{1,5},{5,9},{9,13},{13,1},{2,6},{6,10},{... | collective-permute-start | bytes 2752520 | tf_op jit(solution)/shard_map/ppermute | solution.py:27
  75.2 58.0 %copy-start.11 = (f32[2048]{0:T(1024)S(1)}, f32[2048]{0:T(1024)}, u32[]{:S(2)}) copy-start(f32[2048]{0:T(1024)} %param.15) | copy-start | bytes 24580
  100.6 32.6 %copy-start.3 = (bf16[512,2048]{1,0:T(8,128)(2,1)S(1)}, bf16[512,2048]{1,0:T(8,128)(2,1)}, u32[]{:S(2)}) copy-start(bf16[512,2048]{1,0:T(8,128)(2,1)} %all-gather.9.cloned.1.call-done) | copy-start | bytes 6291460
  215.7 29.9 %copy-start.2 = (bf16[128,2048]{1,0:T(8,128)(2,1)S(1)}, bf16[128,2048]{1,0:T(8,128)(2,1)}, u32[]{:S(2)}) copy-start(bf16[128,2048]{1,0:T(8,128)(2,1)} %param.14) | copy-start | bytes 1572868
  215.7 54.6 %all-gather.15.cloned.1.call-start = ((), (), s32[]{:S(2)}) async-start(), calls=%async_computation.7 | async-start | bytes 2621440 | tf_op jit(solution)/shard_map/all_gather | solution.py:98
  247.6 69.9 %copy-start.12 = (f32[2048]{0:T(1024)S(1)}, f32[2048]{0:T(1024)}, u32[]{:S(2)}) copy-start(f32[2048]{0:T(1024)} %param.20) | copy-start | bytes 24580
  247.6 69.8 %all-gather.19.cloned.1.call-start = ((), (), s32[]{:S(2)}) async-start(), calls=%async_computation.9 | async-start | bytes 2621440 | tf_op jit(solution)/shard_map/all_gather | solution.py:105
  248.2 115.3 %all-gather.17.cloned.1.call-start = ((), (), s32[]{:S(2)}) async-start(), calls=%async_computation.8 | async-start | bytes 2621440 | tf_op jit(solution)/shard_map/all_gather | solution.py:104
  248.9 160.6 %all-gather.21.cloned.1.call-start = ((), (), s32[]{:S(2)}) async-start(), calls=%async_computation.10 | async-start | bytes 2621440 | tf_op jit(solution)/shard_map/all_gather | solution.py:127
  249.7 196.5 %reduce-scatter.6.cloned.1.call-start = ((), (), s32[]{:S(2)}) async-start(), calls=%async_computation.11 | async-start | bytes 2621440 | tf_op jit(solution)/shard_map/reduce_scatter | solution.py:130
  270.3 47.1 %copy-start.4 = (bf16[512,2048]{1,0:T(8,128)(2,1)S(1)}, bf16[512,2048]{1,0:T(8,128)(2,1)}, u32[]{:S(2)}) copy-start(bf16[512,2048]{1,0:T(8,128)(2,1)} %all-gather.15.cloned.1.call-done) | copy-start | bytes 6291460
  272.6 55.7 %copy-start.8 = (f32[512]{0:T(512)S(1)}, f32[512]{0:T(512)}, u32[]{:S(2)}) copy-start(f32[512]{0:T(512)} %param.24) | copy-start | bytes 6148
  272.6 55.7 %copy-start.9 = (f32[512]{0:T(512)S(1)}, f32[512]{0:T(512)}, u32[]{:S(2)}) copy-start(f32[512]{0:T(512)} %param.23) | copy-start | bytes 6148
  321.6 9.1 %copy-start.7 = (bf16[4,128,128]{2,1,0:T(8,128)(2,1)S(1)}, bf16[4,128,128]{2,1,0:T(8,128)(2,1)}, u32[]{:S(2)}) copy-start(bf16[4,128,128]{2,1,0:T(8,128)(2,1)} %param.25) | copy-start | bytes 393220
  321.6 9.1 %copy-start.10 = (f32[4,128]{1,0:T(4,128)S(1)}, f32[4,128]{1,0:T(4,128)}, u32[]{:S(2)}) copy-start(f32[4,128]{1,0:T(4,128)} %param.26) | copy-start | bytes 6148
  416.1 30.2 %copy-start = (bf16[128,2048]{1,0:T(8,128)(2,1)S(1)}, bf16[128,2048]{1,0:T(8,128)(2,1)}, u32[]{:S(2)}) copy-start(bf16[128,2048]{1,0:T(8,128)(2,1)} %add_convert_fusion.3) | copy-start | bytes 1572868
  416.1 57.1 %copy-start.13 = (f32[2048]{0:T(1024)S(1)}, f32[2048]{0:T(1024)}, u32[]{:S(2)}) copy-start(f32[2048]{0:T(1024)} %param.16) | copy-start | bytes 24580
  416.1 54.8 %all-gather.23.cloned.1.call-start = ((), (), s32[]{:S(2)}) async-start(), calls=%async_computation.12 | async-start | bytes 2621440 | tf_op jit(solution)/shard_map/all_gather | solution.py:54
  448.2 71.7 %reduce-scatter.8.cloned.1.call-start = ((), (), s32[]{:S(2)}) async-start(), calls=%async_computation.13 | async-start | bytes 2621440 | tf_op jit(solution)/shard_map/reduce_scatter | solution.py:81
  470.9 2.2 copy-start.5
  488.5 31.4 %copy-start.1 = (bf16[128,2048]{1,0:T(8,128)(2,1)S(1)}, bf16[128,2048]{1,0:T(8,128)(2,1)}, u32[]{:S(2)}) copy-start(bf16[128,2048]{1,0:T(8,128)(2,1)} %add_convert_fusion.1) | copy-start | bytes 1572868
Sparse Core Ops, SparseCore 0:
  8.9 25.2 all-gather.8
  35.8 97.3 all-gather.10
  134.8 71.1 all-gather.12
  215.8 29.7 reduce-scatter.3
  247.7 22.5 all-gather.14
  271.8 45.6 all-gather.18
  319.0 44.4 all-gather.16
  365.1 44.4 all-gather.20
  416.2 29.9 reduce-scatter.5
  448.3 22.5 all-gather.22
  488.6 31.1 reduce-scatter.7
